TPU v7x, 32 devices: a whole 2x2x4 slice. The times are simulated.
32 devices in a mesh: fs: 4 (over z), tp: 4 (over y, x), rep: 2 (over core).
Axes of the slice: x: 2, y: 2, z: 4, core: 2. Of those that a mesh axis runs over, the one named last changes fastest.
Arguments:
- up_weight: float32 [2048, 8192], P('fs', ('tp', 'rep')), may hold values from -0.125 to 0.125
- up_momentum: float32 [2048, 8192], P('fs', ('tp', 'rep')), may hold values from -24 to 24
- up_grads: bfloat16 [2, 2048, 8192], P('rep', 'fs', 'tp'), may hold values from -2.09375 to 2.09375
- out_weight: float32 [2048, 2048], P('fs', ('tp', 'rep')), may hold values from -0.125 to 0.125
- out_momentum: float32 [2048, 2048], P('fs', ('tp', 'rep')), may hold values from -24 to 24
- out_grads: bfloat16 [2, 2048, 2048], P('rep', 'fs', 'tp'), may hold values from -2.09375 to 2.09375
Outputs:
- up_weight_new: float32 [2048, 8192], P('fs', ('tp', 'rep'))
- up_momentum_new: float32 [2048, 8192], P('fs', ('tp', 'rep'))
- up_direction: float32 [2048, 8192], P('fs', ('tp', 'rep'))
- out_weight_new: float32 [2048, 2048], P('fs', ('tp', 'rep'))
- out_momentum_new: float32 [2048, 2048], P('fs', ('tp', 'rep'))
- out_direction: float32 [2048, 2048], P('fs', ('tp', 'rep'))
All inputs are finite; a program needn't handle non-finite values.
Results may differ from a plain program's by a relative error of at most 0.039.
Values may be sent and summed in bfloat16 or wider, within the bound.
A program may use at most 64 MiB of HBM per device.

v0:
```python
import math

import jax
import jax.numpy as jnp
from jax import lax
from jax.sharding import PartitionSpec as P

ITERS = 3


MOMENT = 0.9
RATE = 0.02
COEF_A = 3.4445
COEF_B = -4.775
COEF_C = 2.0315


def local_gram(values, columns):
    return lax.dot_general(
        values, columns, (((1,), (1,)), ((), ())), preferred_element_type=jnp.float32
    )


def contract(gram, values, gram_axis):
    return lax.dot_general(
        gram, values, (((gram_axis,), (0,)), ((), ())), preferred_element_type=jnp.float32
    )


def second_product(gram, first_half, gram_axis):
    return contract(gram, lax.all_gather(first_half, "fs", axis=0, tiled=True), gram_axis)


def on_device(up_weight, up_momentum, up_grads, out_weight, out_momentum, out_grads):
    grad_up, grad_out = (
        lax.psum_scatter(
            up_grads[0].astype(jnp.float32).astype(jnp.bfloat16),
            "rep",
            scatter_dimension=1,
            tiled=True,
        ).astype(jnp.float32),
        lax.psum_scatter(
            out_grads[0].astype(jnp.float32).astype(jnp.bfloat16),
            "rep",
            scatter_dimension=1,
            tiled=True,
        ).astype(jnp.float32),
    )
    moments = [MOMENT * up_momentum + grad_up, MOMENT * out_momentum + grad_out]
    group = lax.axis_size("tp") * lax.axis_size("rep")
    current = moments
    for iteration in range(ITERS):
        values = [entry.astype(jnp.bfloat16) for entry in current]
        columns = (
            lax.all_gather(values[0], "fs", axis=0, tiled=True),
            lax.all_gather(values[1], "fs", axis=0, tiled=True),
        )
        gram_sums = (
            lax.psum(local_gram(values[0], columns[0]).astype(jnp.bfloat16), ("tp", "rep")).astype(
                jnp.float32
            ),
            lax.psum(local_gram(values[1], columns[1]).astype(jnp.bfloat16), ("tp", "rep")).astype(
                jnp.float32
            ),
        )
        gram_axis = 1
        if iteration == 0:
            totals = lax.psum(
                (jnp.sum(gram_sums[0] * gram_sums[0]), jnp.sum(gram_sums[1] * gram_sums[1])), "fs"
            )
        if iteration == 0:
            squares = [1.0 / (jnp.sqrt(total) + 1.0) for total in totals]
            factors = [jnp.sqrt(square) for square in squares]
        else:
            squares = [1.0, 1.0]
            factors = [1.0, 1.0]
        halves = [(gram_sums[index] * squares[index]).astype(jnp.bfloat16) for index in range(2)]
        products = [
            factors[index] * contract(halves[index], columns[index], gram_axis)
            for index in range(2)
        ]
        seconds = [
            second_product(halves[index], products[index].astype(jnp.bfloat16), gram_axis)
            for index in range(2)
        ]
        current = [
            COEF_A * factors[index] * current[index]
            + COEF_B * products[index]
            + COEF_C * seconds[index]
            for index in range(2)
        ]
    widths = [up_weight.shape[1] * group, out_weight.shape[1] * group]
    directions = [current[index] * math.sqrt(widths[index]) for index in range(2)]
    return (
        up_weight - RATE * directions[0],
        moments[0],
        directions[0],
        out_weight - RATE * directions[1],
        moments[1],
        directions[1],
    )


def solution(mesh):
    return jax.shard_map(
        on_device,
        mesh=mesh,
        in_specs=(
            P("fs", ("tp", "rep")),
            P("fs", ("tp", "rep")),
            P("rep", "fs", "tp"),
            P("fs", ("tp", "rep")),
            P("fs", ("tp", "rep")),
            P("rep", "fs", "tp"),
        ),
        out_specs=(
            P("fs", ("tp", "rep")),
            P("fs", ("tp", "rep")),
            P("fs", ("tp", "rep")),
            P("fs", ("tp", "rep")),
            P("fs", ("tp", "rep")),
            P("fs", ("tp", "rep")),
        ),
        check_vma=False,
    )
```

profile of v0, /device:TPU:0, one launch (start us, length us, event | category | flops | bytes accessed | tf_op | source)
XLA Modules:
  0.0 994.7 jit_solution(5314064352922162735)
XLA Ops:
  8.7 12.2 %reduce-scatter.5.cloned.1.call-done = bf16[512,256]{1,0:T(8,128)(2,1)} async-done(((bf16[512,512]{1,0:T(8,128)(2,1)}), bf16[512,256]{1,0:T(8,128)(2,1)}) %reduce-scatter.5.cloned.1.call-update) | async-done | bytes 262160 | tf_op jit(solution)/shard_map/reduce_scatter | solution.py:42
  22.9 11.0 %reduce-scatter.3.cloned.1.call-done = bf16[512,1024]{1,0:T(8,128)(2,1)} async-done(((bf16[512,2048]{1,0:T(8,128)(2,1)}), bf16[512,1024]{1,0:T(8,128)(2,1)}) %reduce-scatter.3.cloned.1.call-update) | async-done | bytes 1048592 | tf_op jit(solution)/shard_map/reduce_scatter | solution.py:36
  33.9 3.3 fusion.26
  37.3 28.1 %all-gather.25.cloned.1.call-done = bf16[2048,256]{1,0:T(8,128)(2,1)} async-done(((bf16[512,256]{1,0:T(8,128)(2,1)}), bf16[2048,256]{1,0:T(8,128)(2,1)}) %all-gather.25.cloned.1.call-update) | async-done | bytes 1048592 | tf_op jit(solution)/shard_map/all_gather | solution.py:56
  68.7 78.9 %all-gather.13.cloned.1.call-done = bf16[2048,1024]{1,0:T(8,128)(2,1)} async-done(((bf16[512,1024]{1,0:T(8,128)(2,1)}), bf16[2048,1024]{1,0:T(8,128)(2,1)}) %all-gather.13.cloned.1.call-update) | async-done | bytes 4194320 | tf_op jit(solution)/shard_map/all_gather | solution.py:55
  147.5 5.9 convolution_convert_fusion.5
  153.5 79.4 %all-reduce.12.cloned.1.call-done = (bf16[512,2048]{1,0:T(8,128)(2,1)}, bf16[512,2048]{1,0:T(8,128)(2,1)}) async-done(((bf16[512,2048]{1,0:T(8,128)(2,1)}, bf16[512,2048]{1,0:T(8,128)(2,1)}), (bf16[512,2048]{1,0:T(8,128)(2,1)}, bf16[512,2048]{1,0:T(8,128)(2,1)})) %all-reduce.12.cloned.1.call-update) | async-done | bytes 4194320 | tf_op jit(solution)/shard_map/psum | solution.py:59
  232.9 4.0 fusion
  236.9 12.3 %all-reduce = (f32[]{:T(128)}, f32[]{:T(128)}) all-reduce(f32[]{:T(128)} %get-tuple-element.42, f32[]{:T(128)} %get-tuple-element.43), channel_id=1, replica_groups=mesh['fs'=4,'tp'=4,'rep'=2] {'fs'}, use_global_device_ids=true, to_apply=%region_3.0 | all-reduce | flops 2 | bytes 16 | tf_op jit(solution)/shard_map/psum | solution.py:68
  250.0 3.3 fusion.28
  254.2 6.3 multiply_convert_fusion
  260.6 18.3 %all-gather.27.cloned.1.call-done = bf16[2048,256]{1,0:T(8,128)(2,1)} async-done(((bf16[512,256]{1,0:T(8,128)(2,1)}), bf16[2048,256]{1,0:T(8,128)(2,1)}) %all-gather.27.cloned.1.call-update) | async-done | bytes 1048592 | tf_op jit(solution)/shard_map/all_gather | solution.py:31
  278.8 3.6 fusion.29
  282.5 78.6 %all-gather.15.cloned.1.call-done = bf16[2048,1024]{1,0:T(8,128)(2,1)} async-done(((bf16[512,1024]{1,0:T(8,128)(2,1)}), bf16[2048,1024]{1,0:T(8,128)(2,1)}) %all-gather.15.cloned.1.call-update) | async-done | bytes 4194320 | tf_op jit(solution)/shard_map/all_gather | solution.py:31
  361.1 7.6 fusion.27
  369.0 20.8 %all-gather.29.cloned.1.call-done = bf16[2048,256]{1,0:T(8,128)(2,1)} async-done(((bf16[512,256]{1,0:T(8,128)(2,1)}), bf16[2048,256]{1,0:T(8,128)(2,1)}) %all-gather.29.cloned.1.call-update) | async-done | bytes 1048592 | tf_op jit(solution)/shard_map/all_gather | solution.py:56
  393.1 79.0 %all-gather.17.cloned.1.call-done = bf16[2048,1024]{1,0:T(8,128)(2,1)} async-done(((bf16[512,1024]{1,0:T(8,128)(2,1)}), bf16[2048,1024]{1,0:T(8,128)(2,1)}) %all-gather.17.cloned.1.call-update) | async-done | bytes 4194320 | tf_op jit(solution)/shard_map/all_gather | solution.py:55
  472.1 5.9 convolution_convert_fusion.4
  478.0 79.4 %all-reduce.10.cloned.1.call-done = (bf16[512,2048]{1,0:T(8,128)(2,1)}, bf16[512,2048]{1,0:T(8,128)(2,1)}) async-done(((bf16[512,2048]{1,0:T(8,128)(2,1)}, bf16[512,2048]{1,0:T(8,128)(2,1)}), (bf16[512,2048]{1,0:T(8,128)(2,1)}, bf16[512,2048]{1,0:T(8,128)(2,1)})) %all-reduce.10.cloned.1.call-update) | async-done | bytes 4194320 | tf_op jit(solution)/shard_map/psum | solution.py:59
  560.6 6.9 fusion.30
  567.6 21.1 %all-gather.31.cloned.1.call-done = bf16[2048,256]{1,0:T(8,128)(2,1)} async-done(((bf16[512,256]{1,0:T(8,128)(2,1)}), bf16[2048,256]{1,0:T(8,128)(2,1)}) %all-gather.31.cloned.1.call-update) | async-done | bytes 1048592 | tf_op jit(solution)/shard_map/all_gather | solution.py:31
  591.6 78.7 %all-gather.19.cloned.1.call-done = bf16[2048,1024]{1,0:T(8,128)(2,1)} async-done(((bf16[512,1024]{1,0:T(8,128)(2,1)}), bf16[2048,1024]{1,0:T(8,128)(2,1)}) %all-gather.19.cloned.1.call-update) | async-done | bytes 4194320 | tf_op jit(solution)/shard_map/all_gather | solution.py:31
  670.3 8.4 fusion.31
  678.7 20.2 %all-gather.33.cloned.1.call-done = bf16[2048,256]{1,0:T(8,128)(2,1)} async-done(((bf16[512,256]{1,0:T(8,128)(2,1)}), bf16[2048,256]{1,0:T(8,128)(2,1)}) %all-gather.33.cloned.1.call-update) | async-done | bytes 1048592 | tf_op jit(solution)/shard_map/all_gather | solution.py:56
  698.9 3.3 convolution_convert_fusion
  702.2 78.3 %all-gather.21.cloned.1.call-done = bf16[2048,1024]{1,0:T(8,128)(2,1)} async-done(((bf16[512,1024]{1,0:T(8,128)(2,1)}), bf16[2048,1024]{1,0:T(8,128)(2,1)}) %all-gather.21.cloned.1.call-update) | async-done | bytes 4194320 | tf_op jit(solution)/shard_map/all_gather | solution.py:55
  780.5 5.9 convolution_convert_fusion.3
  786.4 79.4 %all-reduce.8.cloned.1.call-done = (bf16[512,2048]{1,0:T(8,128)(2,1)}, bf16[512,2048]{1,0:T(8,128)(2,1)}) async-done(((bf16[512,2048]{1,0:T(8,128)(2,1)}, bf16[512,2048]{1,0:T(8,128)(2,1)}), (bf16[512,2048]{1,0:T(8,128)(2,1)}, bf16[512,2048]{1,0:T(8,128)(2,1)})) %all-reduce.8.cloned.1.call-update) | async-done | bytes 4194320 | tf_op jit(solution)/shard_map/psum | solution.py:59
  869.2 7.0 fusion.34
  876.2 20.9 %all-gather.35.cloned.1.call-done = bf16[2048,256]{1,0:T(8,128)(2,1)} async-done(((bf16[512,256]{1,0:T(8,128)(2,1)}), bf16[2048,256]{1,0:T(8,128)(2,1)}) %all-gather.35.cloned.1.call-update) | async-done | bytes 1048592 | tf_op jit(solution)/shard_map/all_gather | solution.py:31
  900.2 78.5 %all-gather.23.cloned.1.call-done = bf16[2048,1024]{1,0:T(8,128)(2,1)} async-done(((bf16[512,1024]{1,0:T(8,128)(2,1)}), bf16[2048,1024]{1,0:T(8,128)(2,1)}) %all-gather.23.cloned.1.call-update) | async-done | bytes 4194320 | tf_op jit(solution)/shard_map/all_gather | solution.py:31
  978.7 9.5 broadcast_multiply_fusion
  (75 shorter events, 23.1 us)
Async XLA Ops:
  7.2 13.7 %reduce-scatter.5.cloned.1.call-start = ((), (), s32[]{:S(2)}) async-start(), calls=%async_computation.9 | async-start | bytes 786432 | tf_op jit(solution)/shard_map/reduce_scatter | solution.py:42
  7.9 26.0 %copy-start.7 = (f32[512,1024]{1,0:T(8,128)S(1)}, f32[512,1024]{1,0:T(8,128)}, u32[]{:S(2)}) copy-start(f32[512,1024]{1,0:T(8,128)} %param.7) | copy-start | bytes 6291460
  7.9 26.0 %reduce-scatter.3.cloned.1.call-start = ((), (), s32[]{:S(2)}) async-start(), calls=%async_computation.2 | async-start | bytes 3145728 | tf_op jit(solution)/shard_map/reduce_scatter | solution.py:36
  8.7 56.7 %all-gather.25.cloned.1.call-start = ((), (), s32[]{:S(2)}) async-start(), calls=%async_computation.10 | async-start | bytes 1310720 | tf_op jit(solution)/shard_map/all_gather | solution.py:56
  22.8 42.6 %copy-start.6 = (bf16[512,256]{1,0:T(8,128)(2,1)S(1)}, bf16[512,256]{1,0:T(8,128)(2,1)}, u32[]{:S(2)}) copy-start(bf16[512,256]{1,0:T(8,128)(2,1)} %get-tuple-element.14) | copy-start | bytes 786436
  22.8 124.7 %all-gather.13.cloned.1.call-start = ((), (), s32[]{:S(2)}) async-start(), calls=%async_computation.3 | async-start | bytes 5242880 | tf_op jit(solution)/shard_map/all_gather | solution.py:55
  37.2 110.3 %copy-start.4 = (bf16[512,1024]{1,0:T(8,128)(2,1)S(1)}, bf16[512,1024]{1,0:T(8,128)(2,1)}, u32[]{:S(2)}) copy-start(bf16[512,1024]{1,0:T(8,128)(2,1)} %get-tuple-element.16) | copy-start | bytes 3145732
  37.3 195.7 %all-reduce.12.cloned.1.call-start = ((), (), s32[]{:S(2)}) async-start(), calls=%async_computation.18 | async-start | bytes 8388608 | tf_op jit(solution)/shard_map/psum | solution.py:59
  153.4 125.4 %all-gather.27.cloned.1.call-start = ((), (), s32[]{:S(2)}) async-start(), calls=%async_computation.11 | async-start | bytes 1310720 | tf_op jit(solution)/shard_map/all_gather | solution.py:31
  232.9 17.1 %copy-start.10 = (bf16[2048,256]{1,0:T(8,128)(2,1)S(1)}, bf16[2048,256]{1,0:T(8,128)(2,1)}, u32[]{:S(2)}) copy-start(bf16[2048,256]{1,0:T(8,128)(2,1)} %all-gather.25.cloned.1.call-done) | copy-start | bytes 3145732
  253.4 107.8 %all-gather.15.cloned.1.call-start = ((), (), s32[]{:S(2)}) async-start(), calls=%async_computation.4 | async-start | bytes 5242880 | tf_op jit(solution)/shard_map/all_gather | solution.py:31
  254.2 24.7 %copy-start.15 = (f32[512,256]{1,0:T(8,128)S(1)}, f32[512,256]{1,0:T(8,128)}, u32[]{:S(2)}) copy-start(f32[512,256]{1,0:T(8,128)} %get-tuple-element.15) | copy-start | bytes 1572868
  254.2 24.6 %copy-start.16 = (f32[512,256]{1,0:T(8,128)S(1)}, f32[512,256]{1,0:T(8,128)}, u32[]{:S(2)}) copy-start(f32[512,256]{1,0:T(8,128)} %get-tuple-element.27) | copy-start | bytes 1572868
  260.5 129.3 %all-gather.29.cloned.1.call-start = ((), (), s32[]{:S(2)}) async-start(), calls=%async_computation.12 | async-start | bytes 1310720 | tf_op jit(solution)/shard_map/all_gather | solution.py:56
  278.8 82.3 %copy-start.8 = (f32[512,1024]{1,0:T(8,128)S(1)}, f32[512,1024]{1,0:T(8,128)}, u32[]{:S(2)}) copy-start(f32[512,1024]{1,0:T(8,128)} %get-tuple-element.17) | copy-start | bytes 6291460
  282.5 189.6 %all-gather.17.cloned.1.call-start = ((), (), s32[]{:S(2)}) async-start(), calls=%async_computation.5 | async-start | bytes 5242880 | tf_op jit(solution)/shard_map/all_gather | solution.py:55
  361.1 28.6 %copy-start.13 = (bf16[512,256]{1,0:T(8,128)(2,1)S(1)}, bf16[512,256]{1,0:T(8,128)(2,1)}, u32[]{:S(2)}) copy-start(bf16[512,256]{1,0:T(8,128)(2,1)} %get-tuple-element.28) | copy-start | bytes 786436
  368.7 103.4 %copy-start.11 = (bf16[512,1024]{1,0:T(8,128)(2,1)S(1)}, bf16[512,1024]{1,0:T(8,128)(2,1)}, u32[]{:S(2)}) copy-start(bf16[512,1024]{1,0:T(8,128)(2,1)} %get-tuple-element.24) | copy-start | bytes 3145732
  368.7 188.7 %all-reduce.10.cloned.1.call-start = ((), (), s32[]{:S(2)}) async-start(), calls=%async_computation.17 | async-start | bytes 8388608 | tf_op jit(solution)/shard_map/psum | solution.py:59
  477.9 79.5 %copy-start.2 = (bf16[2048,256]{1,0:T(8,128)(2,1)S(1)}, bf16[2048,256]{1,0:T(8,128)(2,1)}, u32[]{:S(2)}) copy-start(bf16[2048,256]{1,0:T(8,128)(2,1)} %all-gather.29.cloned.1.call-done) | copy-start | bytes 3145732
  478.0 110.7 %all-gather.31.cloned.1.call-start = ((), (), s32[]{:S(2)}) async-start(), calls=%async_computation.13 | async-start | bytes 1310720 | tf_op jit(solution)/shard_map/all_gather | solution.py:31
  560.5 109.8 %all-gather.19.cloned.1.call-start = ((), (), s32[]{:S(2)}) async-start(), calls=%async_computation.6 | async-start | bytes 5242880 | tf_op jit(solution)/shard_map/all_gather | solution.py:31
  560.5 28.2 %copy-start = (bf16[512,2048]{1,0:T(8,128)(2,1)S(1)}, bf16[512,2048]{1,0:T(8,128)(2,1)}, u32[]{:S(2)}) copy-start(bf16[512,2048]{1,0:T(8,128)(2,1)} %get-tuple-element.11) | copy-start | bytes 6291460
  567.5 131.4 %all-gather.33.cloned.1.call-start = ((), (), s32[]{:S(2)}) async-start(), calls=%async_computation.14 | async-start | bytes 1310720 | tf_op jit(solution)/shard_map/all_gather | solution.py:56
  591.5 189.0 %all-gather.21.cloned.1.call-start = ((), (), s32[]{:S(2)}) async-start(), calls=%async_computation.7 | async-start | bytes 5242880 | tf_op jit(solution)/shard_map/all_gather | solution.py:55
  670.3 28.6 %copy-start.5 = (bf16[512,256]{1,0:T(8,128)(2,1)S(1)}, bf16[512,256]{1,0:T(8,128)(2,1)}, u32[]{:S(2)}) copy-start(bf16[512,256]{1,0:T(8,128)(2,1)} %get-tuple-element.36) | copy-start | bytes 786436
  678.6 101.9 %copy-start.12 = (bf16[512,1024]{1,0:T(8,128)(2,1)S(1)}, bf16[512,1024]{1,0:T(8,128)(2,1)}, u32[]{:S(2)}) copy-start(bf16[512,1024]{1,0:T(8,128)(2,1)} %get-tuple-element.32) | copy-start | bytes 3145732
  678.6 187.2 %all-reduce.8.cloned.1.call-start = ((), (), s32[]{:S(2)}) async-start(), calls=%async_computation.16 | async-start | bytes 8388608 | tf_op jit(solution)/shard_map/psum | solution.py:59
  786.4 79.5 %copy-start.3 = (bf16[2048,256]{1,0:T(8,128)(2,1)S(1)}, bf16[2048,256]{1,0:T(8,128)(2,1)}, u32[]{:S(2)}) copy-start(bf16[2048,256]{1,0:T(8,128)(2,1)} %all-gather.33.cloned.1.call-done) | copy-start | bytes 3145732
  786.4 110.7 %all-gather.35.cloned.1.call-start = ((), (), s32[]{:S(2)}) async-start(), calls=%async_computation.15 | async-start | bytes 1310720 | tf_op jit(solution)/shard_map/all_gather | solution.py:31
  868.9 109.8 %all-gather.23.cloned.1.call-start = ((), (), s32[]{:S(2)}) async-start(), calls=%async_computation.8 | async-start | bytes 5242880 | tf_op jit(solution)/shard_map/all_gather | solution.py:31
  869.2 27.9 %copy-start.1 = (bf16[512,2048]{1,0:T(8,128)(2,1)S(1)}, bf16[512,2048]{1,0:T(8,128)(2,1)}, u32[]{:S(2)}) copy-start(bf16[512,2048]{1,0:T(8,128)(2,1)} %get-tuple-element.9) | copy-start | bytes 6291460
  (2 other events, 17.9 us)
Sparse Core Ops, SparseCore 0:
  10.2 10.6 reduce-scatter.4
  23.1 10.7 reduce-scatter.2
  36.1 29.2 all-gather.24
  67.4 80.1 all-gather.12
  153.5 79.3 all-reduce.11
  253.5 25.3 all-gather.26
  281.0 80.1 all-gather.14
  363.3 26.4 all-gather.28
  391.9 80.1 all-gather.16
  478.1 79.3 all-reduce.9
  560.6 28.0 all-gather.30
  590.1 80.1 all-gather.18
  672.4 26.4 all-gather.32
  700.3 80.0 all-gather.20
  786.5 79.3 all-reduce.7
  869.0 28.0 all-gather.34
  898.5 80.1 all-gather.22
where the time goes:
time: 995 us
  waiting for transfers between devices  864 us (87%)
  matrix products  91.9 us (9%)
  between operations  15.6 us (2%)
  blocking collectives  12.3 us (1%)
    all_gather x6, waiting for transfers between devices, second_product(): lax.all_gather(first_half, 'fs', axis=0, tiled=True)  296 us
    psum x3, waiting for transfers between devices, on_device(): lax.psum(local_gram(values[0], columns[0]).astype(jnp.bfloat16), ('tp', '...  238 us
    all_gather x3, waiting for transfers between devices, on_device(): lax.all_gather(values[0], 'fs', axis=0, tiled=True)  236 us
    all_gather x3, waiting for transfers between devices, on_device(): lax.all_gather(values[1], 'fs', axis=0, tiled=True)  69.1 us
    dot_general x12, matrix products, contract(): lax.dot_general(gram, values, (((gram_axis,), (0,)), ((), ())), preferred...  64.4 us
    dot_general x6, matrix products, local_gram(): lax.dot_general(values, columns, (((1,), (1,)), ((), ())), preferred_elem...  27.5 us
  transfers between devices with their start and end apart: 17, of which 17 were waited for; matrix products, arithmetic and copies ran while one was open for 6% of the time, Pallas kernels for 0%

commit v1 on v0

v1 whole, which is shorter than its diff:
```python
import math

import jax
import jax.numpy as jnp
from jax import lax
from jax.sharding import PartitionSpec as P

ITERS = 3
MOMENT = 0.9
RATE = 0.02
COEF_A = 3.4445
COEF_B = -4.775
COEF_C = 2.0315
BF = jnp.bfloat16
F32 = jnp.float32
ROLES = 2
CUTS = 8


def mm(a, b):
    return jnp.dot(a, b, preferred_element_type=F32)


def mm_t(a, b):
    return lax.dot_general(a, b, (((1,), (1,)), ((), ())), preferred_element_type=F32)


def reduced_grad(grads):
    size = lax.axis_size("rep")
    rows, cols = grads.shape
    pieces = grads.reshape(rows, size, cols // size).transpose(1, 0, 2)
    pieces = lax.all_to_all(pieces, "rep", split_axis=0, concat_axis=0, tiled=True)
    return jnp.sum(pieces.astype(F32), axis=0)


def to_columns(values):
    size = lax.axis_size("fs")
    rows, cols = values.shape
    pieces = values.reshape(rows, size, cols // size).transpose(1, 0, 2)
    pieces = lax.all_to_all(pieces, "fs", split_axis=0, concat_axis=0, tiled=True)
    return pieces.reshape(size * rows, cols // size)


def to_rows(values):
    size = lax.axis_size("fs")
    rows, cols = values.shape
    pieces = values.reshape(size, rows // size, cols)
    pieces = lax.all_to_all(pieces, "fs", split_axis=0, concat_axis=0, tiled=True)
    return pieces.transpose(1, 0, 2).reshape(rows // size, cols * size)


def swap_pairs(values):
    size = lax.axis_size("rep")
    return lax.ppermute(values, "rep", [(i, i ^ 1) for i in range(size)])


def pack_gram(x):
    step = x.shape[0] // CUTS
    rows = []
    for i in range(CUTS // 2):
        j = CUTS - 1 - i
        rows.append(
            jnp.concatenate(
                [
                    mm_t(x[i * step : (i + 1) * step], x[i * step :]).astype(BF),
                    mm_t(x[j * step : (j + 1) * step], x[j * step :]).astype(BF),
                ],
                axis=1,
            )
        )
    return jnp.concatenate(rows, axis=0)


def unpack_gram(packed):
    step = packed.shape[0] * 2 // CUTS
    upper = {}
    for i in range(CUTS // 2):
        row = packed[i * step : (i + 1) * step]
        upper[i] = row[:, : (CUTS - i) * step]
        upper[CUTS - 1 - i] = row[:, (CUTS - i) * step :]
    full = []
    for i in range(CUTS):
        left = [upper[j][:, (i - j) * step : (i - j + 1) * step].T for j in range(i)]
        full.append(jnp.concatenate(left + [upper[i]], axis=1))
    return jnp.concatenate(full, axis=0)


def next_gram(a):
    square = mm(a, a)
    q = (COEF_B * a.astype(F32) + COEF_C * square).astype(BF)
    w = (COEF_A * a.astype(F32) + mm(q, a)).astype(BF)
    return (COEF_A * w.astype(F32) + mm(q, w)).astype(BF)


def on_device(up_weight, up_momentum, up_grads, out_weight, out_momentum, out_grads):
    even = lax.axis_index("rep") % 2 == 0
    up_moment = MOMENT * up_momentum + reduced_grad(up_grads[0])
    out_moment = MOMENT * out_momentum + reduced_grad(out_grads[0])
    up = to_columns(up_moment.astype(BF))
    out = to_columns(out_moment.astype(BF))
    width, narrow = up.shape[1], out.shape[1]
    out = jnp.pad(out, ((0, 0), (0, width - narrow)))
    other = swap_pairs(jnp.where(even, out, up))
    values = jnp.concatenate([jnp.where(even, up, out), other], axis=1)
    gram = unpack_gram(lax.psum(pack_gram(values), ("fs", "tp"))) if lax.axis_size("rep") == 2 else None
    if gram is None:
        size = lax.axis_size("rep")
        groups = [[i for i in range(size) if i % 2 == k] for k in range(2)]
        packed = lax.psum(pack_gram(values), ("fs", "tp"))
        packed = lax.psum(packed, "rep", axis_index_groups=groups)
        gram = unpack_gram(packed)
    gram = gram.astype(F32)
    square = 1.0 / (jnp.sqrt(jnp.sum(gram * gram)) + 1.0)
    factor = jnp.sqrt(square)
    a = (gram * square).astype(BF)
    current = values.astype(F32)
    for iteration in range(ITERS):
        y = mm(a, current.astype(BF))
        if iteration == 0:
            y = factor * y
            current = factor * current
        z = mm(a, y.astype(BF))
        current = COEF_A * current + COEF_B * y + COEF_C * z
        if iteration < ITERS - 1:
            a = next_gram(a)
    final = current.astype(BF)
    mine, other = final[:, :width], swap_pairs(final[:, width:])
    up = to_rows(jnp.where(even, mine, other)).astype(F32)
    out = to_rows(jnp.where(even, other, mine)[:, :narrow]).astype(F32)
    group = lax.axis_size("tp") * lax.axis_size("rep")
    up_direction = up * math.sqrt(up_weight.shape[1] * group)
    out_direction = out * math.sqrt(out_weight.shape[1] * group)
    return (
        up_weight - RATE * up_direction,
        up_moment,
        up_direction,
        out_weight - RATE * out_direction,
        out_moment,
        out_direction,
    )


def solution(mesh):
    flat = P("fs", ("tp", "rep"))
    grads = P("rep", "fs", "tp")
    return jax.shard_map(
        on_device,
        mesh=mesh,
        in_specs=(flat, flat, grads, flat, flat, grads),
        out_specs=(flat,) * 6,
        check_vma=False,
    )
```

time: 995 us -> 541 us (0.54)
  waiting for transfers between devices: 864 us -> 229 us
  matrix products: 91.9 us -> 182 us
  local copies, waits for them, and re-layouts: 0.07 us -> 40.1 us
  other arithmetic: 9.21 us -> 35.2 us
  starting transfers between devices: 1.1 us -> 20.8 us
    all_gather x12 -> x0, waiting for transfers between devices: 601 us -> none  [the longest x6 296 us: second_product(): lax.all_gather(first_half, 'fs', axis=0, tiled=True)]
    dot_general x18 -> x20, matrix products: 91.9 us -> 182 us  [the longest x12 178 us: mm(): return jnp.dot(a, b, preferred_element_type=F32)]
    psum x3 -> x1, waiting for transfers between devices: 238 us -> 178 us  [on_device(): lax.psum(pack_gram(values), ('fs', 'tp'))]
    all_to_all x0 -> x5, waiting for transfers between devices: none -> 45.7 us  [the longest x2 28.1 us: to_columns(): lax.all_to_all(pieces, 'fs', split_axis=0, concat_axis=0, tiled=True)]
    unnamed x34 -> x95, local copies, waits for them, and re-layouts: 0.07 us -> 24.6 us
    reduce_scatter x2 -> x0, waiting for transfers between devices: 23.2 us -> none  [the longest x1 12.2 us: on_device(): lax.psum_scatter(out_grads[0].astype(jnp.float32).astype(jnp.bfloat16), '...]
    all_to_all x0 -> x5, starting transfers between devices: none -> 20.6 us  [the longest x2 9.86 us: to_columns(): lax.all_to_all(pieces, 'fs', split_axis=0, concat_axis=0, tiled=True)]
    concatenate x0 -> x1, other arithmetic: none -> 18.5 us  [pack_gram(): return jnp.concatenate(rows, axis=0)]
  transfers between devices with their start and end apart: 17 -> 8, of which waited for: 17 -> 7; matrix products, arithmetic and copies ran while one was open for 6% -> 4% of each run, Pallas kernels for 0% -> 0%
where the time goes in v1:
time: 541 us; the launch traced here: 535 us
  waiting for transfers between devices  229 us (42%)
  matrix products  182 us (34%)
  local copies, waits for them, and re-layouts  40.1 us (7%)
  other arithmetic  35.2 us (7%)
  starting transfers between devices  20.8 us (4%)
  between operations  16 us (3%)
  blocking collectives  11.9 us (2%)
    psum x1, waiting for transfers between devices, on_device(): lax.psum(pack_gram(values), ('fs', 'tp'))  178 us
    dot_general x12, matrix products, mm(): return jnp.dot(a, b, preferred_element_type=F32)  178 us
    all_to_all x2, waiting for transfers between devices, to_columns(): lax.all_to_all(pieces, 'fs', split_axis=0, concat_axis=0, tiled=True)  28.1 us
    unnamed x95, local copies, waits for them, and re-layouts  24.6 us
    concatenate x1, other arithmetic, pack_gram(): return jnp.concatenate(rows, axis=0)  18.5 us
    all_to_all x1, waiting for transfers between devices, to_rows(): lax.all_to_all(pieces, 'fs', split_axis=0, concat_axis=0, tiled=True)  16.5 us
    all_to_all x1, blocking collectives, to_rows(): lax.all_to_all(pieces, 'fs', split_axis=0, concat_axis=0, tiled=True)  11.9 us
  transfers between devices with their start and end apart: 8, of which 7 were waited for; matrix products, arithmetic and copies ran while one was open for 4% of the time, Pallas kernels for 0%

profile of v1, /device:TPU:0, one launch (start us, length us, event | category | flops | bytes accessed | tf_op | source)
XLA Modules:
  0.0 534.9 jit_solution(14960733986047631695)
XLA Ops:
  9.5 3.5 all-to-all-start.2
  13.0 2.9 copy.125
  15.9 2.4 copy.126
  18.2 3.8 all-to-all-start
  24.9 6.3 %all-to-all-start.3 = ((bf16[4,512,64]{1,2,0:T(8,128)(2,1)}), bf16[4,512,64]{1,2,0:T(8,128)(2,1)S(1)}, u32[]{:S(2)}, u32[]{:S(2)}) async-start(bf16[4,512,64]{1,2,0:T(8,128)(2,1)} %bitcast.7), calls=%async_computation.3 | async-start | bytes 524288 | tf_op jit(solution)/shard_map/all_to_all | solution.py:40
  31.7 3.4 fusion.64
  36.2 4.3 all-to-all-done.3
  40.4 3.5 all-to-all-start.1
  44.3 23.9 %all-to-all-done.1 = bf16[4,512,256]{2,1,0:T(8,128)(2,1)S(1)} async-done(((bf16[4,512,256]{2,1,0:T(8,128)(2,1)}), bf16[4,512,256]{2,1,0:T(8,128)(2,1)S(1)}, u32[]{:S(2)}, u32[]{:S(2)}) %all-to-all-start.1) | async-done | bytes 1048608 | tf_op jit(solution)/shard_map/all_to_all | solution.py:40
  68.7 2.6 collective-permute-done
  75.4 18.5 %maximum_maximum_fusion = bf16[1024,2304]{1,0:T(8,128)(2,1)} fusion(bf16[256,1024]{1,0:T(8,128)(2,1)S(1)} %convolution_convert_fusion.4, bf16[256,1280]{1,0:T(8,128)(2,1)S(1)} %convolution_convert_fusion.2, bf16[256,768]{1,0:T(8,128)(2,1)S(1)} %convolution_convert_fusion.5, bf16[256,1536]{1,0:T(8,128)(2,1)S(1)} %convolution_convert_fusion.3, ...), kind=kLoop, calls=%fused_computation.49 | loop fusion | flops 37748736 | bytes 9437184 | tf_op jit(solution)/shard_map/concatenate | solution.py:71
  93.9 178.2 %all-reduce.3.cloned.1.call-done = bf16[1024,2304]{1,0:T(8,128)(2,1)} async-done(((bf16[1024,2304]{1,0:T(8,128)(2,1)}), bf16[1024,2304]{1,0:T(8,128)(2,1)}) %all-reduce.3.cloned.1.call-update) | async-done | bytes 4718608 | tf_op jit(solution)/shard_map/psum | solution.py:105
  292.9 3.2 copy-done.4
  296.1 4.9 fusion
  301.8 26.9 %fusion.5 = bf16[2048,2048]{1,0:T(8,128)(2,1)} fusion(f32[]{:T(128)S(6)} %div.3, bf16[2048,2048]{1,0:T(8,128)(2,1)} %copy-done.4), kind=kOutput, calls=%fused_computation.11 | convolution fusion | flops 17226006528 | bytes 16777220 | tf_op jit(solution)/shard_map/dot_general | solution.py:21
  328.7 21.5 %fusion.3 = bf16[2048,2048]{1,0:T(8,128)(2,1)} fusion(bf16[2048,2048]{1,0:T(8,128)(2,1)} %fusion.5, f32[]{:T(128)S(6)} %div.3, bf16[2048,2048]{1,0:T(8,128)(2,1)S(1)} %copy-done.5), kind=kOutput, calls=%fused_computation.9 | convolution fusion | flops 17221812224 | bytes 25165828 | tf_op jit(solution)/shard_map/dot_general | solution.py:21
  350.2 26.4 %add_convert_fusion.1 = bf16[2048,2048]{1,0:T(8,128)(2,1)} fusion(bf16[2048,2048]{1,0:T(8,128)(2,1)} %fusion.3, bf16[2048,2048]{1,0:T(8,128)(2,1)} %fusion.5), kind=kOutput, calls=%fused_computation.17 | convolution fusion | flops 17196646400 | bytes 25165824 | tf_op jit(solution)/shard_map/dot_general | solution.py:21
  376.6 26.6 %fusion.9 = bf16[2048,2048]{1,0:T(8,128)(2,1)} fusion(bf16[2048,2048]{1,0:T(8,128)(2,1)} %add_convert_fusion.1), kind=kOutput, calls=%fused_computation.15 | convolution fusion | flops 17200840704 | bytes 16777216 | tf_op jit(solution)/shard_map/dot_general | solution.py:21
  403.2 4.6 fusion.14
  407.8 5.4 %multiply_add_fusion.1 = f32[2048,512]{1,0:T(8,128)S(1)} fusion(f32[2048,512]{1,0:T(8,128)S(1)} %fusion.14, bf16[2048,2048]{1,0:T(8,128)(2,1)S(1)} %copy-done.5, f32[]{:T(128)S(6)} %div.3, f32[]{:T(128)S(6)} %sqrt.7, bf16[2048,256]{1,0:T(8,128)(2,1)S(1)} %copy-done.3, bf16[2048,256]{1,0:T(8,128)(2,1)S(1)} %copy-done.1), kind=kOutput, calls=%fused_computation.52 | convolution fusion | flops 4321181696 | bytes 18874376 | tf_op jit(solution)/shard_map/dot_general | solution.py:21
  413.2 7.6 %fusion.24 = f32[2048,512]{1,0:T(8,128)S(1)} fusion(bf16[2048,2048]{1,0:T(8,128)(2,1)} %add_convert_fusion.1, f32[2048,512]{1,0:T(8,128)S(1)} %multiply_add_fusion.1), kind=kOutput, calls=%fused_computation.67 | convolution fusion | flops 4296015872 | bytes 16777216 | tf_op jit(solution)/shard_map/dot_general | solution.py:21
  420.9 7.7 %multiply_add_fusion = f32[2048,512]{1,0:T(8,128)S(1)} fusion(f32[2048,512]{1,0:T(8,128)S(1)} %fusion.24, f32[2048,512]{1,0:T(8,128)S(1)} %multiply_add_fusion.1, bf16[2048,2048]{1,0:T(8,128)(2,1)} %add_convert_fusion.1), kind=kOutput, calls=%fused_computation.51 | convolution fusion | flops 4301258752 | bytes 20971520 | tf_op jit(solution)/shard_map/dot_general | solution.py:21
  428.6 20.1 %fusion.7 = bf16[2048,2048]{1,0:T(8,128)(2,1)S(1)} fusion(bf16[2048,2048]{1,0:T(8,128)(2,1)S(1)} %bitcast.115, bf16[2048,2048]{1,0:T(8,128)(2,1)} %fusion.9), kind=kOutput, calls=%fused_computation.13 | convolution fusion | flops 17196646400 | bytes 25165824 | tf_op jit(solution)/shard_map/dot_general | solution.py:21
  448.7 20.3 %add_convert_fusion = bf16[2048,2048]{1,0:T(8,128)(2,1)S(1)} fusion(bf16[2048,2048]{1,0:T(8,128)(2,1)S(1)} %fusion.7, bf16[2048,2048]{1,0:T(8,128)(2,1)} %fusion.9), kind=kOutput, calls=%fused_computation.16 | convolution fusion | flops 17196646400 | bytes 25165824 | tf_op jit(solution)/shard_map/dot_general | solution.py:21
  469.0 4.5 fusion.21
  473.6 6.0 %add_convert_fusion.2 = bf16[2048,512]{1,0:T(8,128)(2,1)S(1)} fusion(f32[2048,512]{1,0:T(8,128)S(1)} %fusion.21, f32[2048,512]{1,0:T(8,128)S(1)} %multiply_add_fusion, bf16[2048,2048]{1,0:T(8,128)(2,1)S(1)} %add_convert_fusion), kind=kOutput, calls=%fused_computation.50 | convolution fusion | flops 4302307328 | bytes 18874368 | tf_op jit(solution)/shard_map/dot_general | solution.py:21
  479.8 2.6 collective-permute-done.1
  483.8 11.9 %all_to_all.30 = bf16[4,512,64]{1,2,0:T(8,128)(2,1)S(1)} all-to-all(bf16[4,512,64]{1,2,0:T(8,128)(2,1)S(1)} %copy.164), channel_id=1, replica_groups=mesh['fs'=4,'tp'=4,'rep'=2] {'fs'}, dimensions={0} | all-to-all | bytes 524288 | tf_op jit(solution)/shard_map/all_to_all | solution.py:48
  495.7 3.5 all-to-all-start.4
  501.1 2.0 bitcast_subtract_fusion
  503.1 2.0 copy.166
  507.2 16.5 %all-to-all-done.4 = bf16[4,512,256]{2,1,0:T(8,128)(2,1)S(1)} async-done(((bf16[4,512,256]{2,1,0:T(8,128)(2,1)}), bf16[4,512,256]{2,1,0:T(8,128)(2,1)S(1)}, u32[]{:S(2)}, u32[]{:S(2)}) %all-to-all-start.4) | async-done | bytes 1048608 | tf_op jit(solution)/shard_map/all_to_all | solution.py:48
  (133 shorter events, 41.2 us)
Async XLA Ops:
  7.2 14.9 %copy-start.7 = (f32[512,256]{1,0:T(8,128)S(1)}, f32[512,256]{1,0:T(8,128)}, u32[]{:S(2)}) copy-start(f32[512,256]{1,0:T(8,128)} %param.10) | copy-start | bytes 1572868
  9.5 8.8 %all-to-all-start.2 = ((bf16[2,512,256]{2,1,0:T(8,128)(2,1)}), bf16[2,512,256]{2,1,0:T(8,128)(2,1)S(1)}, u32[]{:S(2)}, u32[]{:S(2)}) async-start(bf16[2,512,256]{2,1,0:T(8,128)(2,1)} %copy.129), calls=%async_computation.2 | async-start | bytes 1048576 | tf_op jit(solution)/shard_map/all_to_all | solution.py:32
  18.2 6.6 %all-to-all-start = ((bf16[2,512,1024]{2,1,0:T(8,128)(2,1)}), bf16[2,512,1024]{2,1,0:T(8,128)(2,1)S(1)}, u32[]{:S(2)}, u32[]{:S(2)}) async-start(bf16[2,512,1024]{2,1,0:T(8,128)(2,1)} %copy.126), calls=%async_computation | async-start | bytes 4194304 | tf_op jit(solution)/shard_map/all_to_all | solution.py:32
  24.9 15.6 %all-to-all-start.3 = ((bf16[4,512,64]{1,2,0:T(8,128)(2,1)}), bf16[4,512,64]{1,2,0:T(8,128)(2,1)S(1)}, u32[]{:S(2)}, u32[]{:S(2)}) async-start(bf16[4,512,64]{1,2,0:T(8,128)(2,1)} %bitcast.7), calls=%async_computation.3 | async-start | bytes 524288 | tf_op jit(solution)/shard_map/all_to_all | solution.py:40
  40.4 27.7 %all-to-all-start.1 = ((bf16[4,512,256]{2,1,0:T(8,128)(2,1)}), bf16[4,512,256]{2,1,0:T(8,128)(2,1)S(1)}, u32[]{:S(2)}, u32[]{:S(2)}) async-start(bf16[4,512,256]{2,1,0:T(8,128)(2,1)} %bitcast.99), calls=%async_computation.1 | async-start | bytes 2097152 | tf_op jit(solution)/shard_map/all_to_all | solution.py:40
  44.0 228.1 %all-reduce.3.cloned.1.call-start = ((), (), s32[]{:S(2)}) async-start(), calls=%async_computation.6 | async-start | bytes 9437184 | tf_op jit(solution)/shard_map/psum | solution.py:105
  68.6 6.3 %copy-start = (bf16[2048,256]{1,0:T(8,128)(2,1)}, bf16[2048,256]{1,0:T(8,128)(2,1)S(1)}, u32[]{:S(2)}) copy-start(bf16[2048,256]{1,0:T(8,128)(2,1)S(1)} %get-tuple-element.59) | copy-start | bytes 3145732
  68.6 2.7 collective-permute-start
  71.3 3.6 copy-start.2
  280.8 7.5 %copy-start.9 = (bf16[256,256]{0,1:T(8,128)(2,1)S(1)}, bf16[256,256]{0,1:T(8,128)(2,1)}, u32[]{:S(2)}) copy-start(bf16[256,256]{0,1:T(8,128)(2,1)} %copy.176) | copy-start | bytes 393220
  282.4 7.1 %copy-start.13 = (bf16[256,256]{0,1:T(8,128)(2,1)S(1)}, bf16[256,256]{0,1:T(8,128)(2,1)}, u32[]{:S(2)}) copy-start(bf16[256,256]{0,1:T(8,128)(2,1)} %copy.181) | copy-start | bytes 393220
  282.6 7.0 %copy-start.12 = (bf16[256,256]{0,1:T(8,128)(2,1)S(1)}, bf16[256,256]{0,1:T(8,128)(2,1)}, u32[]{:S(2)}) copy-start(bf16[256,256]{0,1:T(8,128)(2,1)} %copy.182) | copy-start | bytes 393220
  282.7 6.9 %copy-start.11 = (bf16[256,256]{0,1:T(8,128)(2,1)S(1)}, bf16[256,256]{0,1:T(8,128)(2,1)}, u32[]{:S(2)}) copy-start(bf16[256,256]{0,1:T(8,128)(2,1)} %copy.183) | copy-start | bytes 393220
  282.8 6.8 %copy-start.10 = (bf16[256,256]{0,1:T(8,128)(2,1)S(1)}, bf16[256,256]{0,1:T(8,128)(2,1)}, u32[]{:S(2)}) copy-start(bf16[256,256]{0,1:T(8,128)(2,1)} %copy.184) | copy-start | bytes 393220
  283.0 5.4 %copy-start.15 = (bf16[256,256]{0,1:T(8,128)(2,1)S(1)}, bf16[256,256]{0,1:T(8,128)(2,1)}, u32[]{:S(2)}) copy-start(bf16[256,256]{0,1:T(8,128)(2,1)} %copy.179) | copy-start | bytes 393220
  283.0 6.5 %copy-start.14 = (bf16[256,256]{0,1:T(8,128)(2,1)S(1)}, bf16[256,256]{0,1:T(8,128)(2,1)}, u32[]{:S(2)}) copy-start(bf16[256,256]{0,1:T(8,128)(2,1)} %copy.180) | copy-start | bytes 393220
  292.8 3.2 copy-start.4
  301.8 26.9 %copy-start.5 = (bf16[2048,2048]{1,0:T(8,128)(2,1)S(1)}, bf16[2048,2048]{1,0:T(8,128)(2,1)}, u32[]{:S(2)}) copy-start(bf16[2048,2048]{1,0:T(8,128)(2,1)} %copy-done.4) | copy-start | bytes 25165828
  376.6 26.6 %copy-start.1 = (bf16[2048,256]{1,0:T(8,128)(2,1)S(1)}, bf16[2048,256]{1,0:T(8,128)(2,1)}, u32[]{:S(2)}) copy-start(bf16[2048,256]{1,0:T(8,128)(2,1)} %copy-done) | copy-start | bytes 3145732
  376.6 26.6 %copy-start.3 = (bf16[2048,256]{1,0:T(8,128)(2,1)S(1)}, bf16[2048,256]{1,0:T(8,128)(2,1)}, u32[]{:S(2)}) copy-start(bf16[2048,256]{1,0:T(8,128)(2,1)} %copy-done.2) | copy-start | bytes 3145732
  413.2 15.4 %slice-start = ((s8[8388608]{0:T(1024)(128)(4,1)}), s8[4194304]{0:T(1024)(128)(4,1)S(1)}, s32[]{:S(2)}) async-start(s8[8388608]{0:T(1024)(128)(4,1)} %bitcast.114), calls=%async_computation.7 | async-start | bytes 8388608
  420.8 7.8 %slice-start.1 = ((s8[8388608]{0:T(1024)(128)(4,1)}), s8[4194304]{0:T(1024)(128)(4,1)S(1)}, s32[]{:S(2)}) async-start(s8[8388608]{0:T(1024)(128)(4,1)} %bitcast.114), calls=%async_computation.8 | async-start | bytes 8388608
  479.6 19.6 %copy-start.8 = (f32[512,256]{1,0:T(8,128)S(1)}, f32[512,256]{1,0:T(8,128)}, u32[]{:S(2)}) copy-start(f32[512,256]{1,0:T(8,128)} %param.9) | copy-start | bytes 1572868
  479.7 2.7 collective-permute-start.1
  495.7 28.0 %all-to-all-start.4 = ((bf16[4,512,256]{2,1,0:T(8,128)(2,1)}), bf16[4,512,256]{2,1,0:T(8,128)(2,1)S(1)}, u32[]{:S(2)}, u32[]{:S(2)}) async-start(bf16[4,512,256]{2,1,0:T(8,128)(2,1)} %bitcast.37), calls=%async_computation.4 | async-start | bytes 2097152 | tf_op jit(solution)/shard_map/all_to_all | solution.py:48
  501.1 25.0 %copy-start.6 = (f32[512,1024]{1,0:T(8,128)S(1)}, f32[512,1024]{1,0:T(8,128)}, u32[]{:S(2)}) copy-start(f32[512,1024]{1,0:T(8,128)} %param.6) | copy-start | bytes 6291460
Sparse Core Ops, SparseCore 0:
  94.0 178.0 all-reduce.2
